TPU v7x, 32 devices: a whole 2x2x4 slice. The times are simulated.
32 devices in a mesh: row: 8 (over z, y), col: 4 (over x, core).
Axes of the slice: x: 2, y: 2, z: 4, core: 2. Of those that a mesh axis runs over, the one named last changes fastest.
Arguments:
- tokens: bfloat16 [2, 16384, 1024], P(None, 'row'), may hold values from -6 to 6
- norm_gain: float32 [1024], replicated, may hold values from 0.1 to 1.9
- w_fourier_in: bfloat16 [1024, 512], P(None, 'col'), may hold values from -0.1875 to 0.1875
- w_gate: bfloat16 [1024, 1024], replicated, may hold values from -0.1875 to 0.1875
- w_spectrum: bfloat16 [512, 1024], replicated, may hold values from -0.25 to 0.25
- w_output: bfloat16 [1024, 1024], P(None, 'col'), may hold values from -0.375 to 0.375
Outputs:
- block_output: bfloat16 [2, 16384, 1024], P(None, 'row', 'col')
All inputs are finite; a program needn't handle non-finite values.
Results may differ from a plain program's by a relative error of at most 0.015.
Values may be sent and summed in bfloat16 or wider, within the bound.
A program may use at most 320 MiB of HBM per device.

v0:
```python
import functools

import jax
import jax.numpy as jnp
import numpy as np
from jax import lax
from jax.experimental import pallas as pl
from jax.experimental.pallas import tpu as pltpu
from jax.sharding import PartitionSpec as P

GROUP_WIDTH = 64
FIRST_LEN = 256


norm_eps = 1e-06


def shortened(value):
    return jax.tree.map(lambda a: a.astype(jnp.bfloat16) if a.dtype == jnp.float32 else a, value)


def over_all(value, axis, dim, absorb, carry):
    whole = jax.tree.map(lambda part: lax.all_gather(part, axis, axis=dim, tiled=True), value)
    return absorb(carry, whole, jnp.int32(0))


def dft_tables(length_in, length_out, period):
    left_index = lax.broadcasted_iota(jnp.int32, (length_in, length_out), 0)
    right_index = lax.broadcasted_iota(jnp.int32, (length_in, length_out), 1)
    angles = (left_index * right_index % period).astype(jnp.float32) * (2.0 * jnp.pi / period)
    return (jnp.cos(angles), jnp.sin(angles))


def transform_first(cube, table):
    return jnp.einsum("cpq,pk->ckq", cube, table, precision=lax.Precision.HIGHEST)


def transform_second(cube, table):
    return jnp.einsum("ckq,qj->cjk", cube, table, precision=lax.Precision.HIGHEST)


def positional(real_part, imag_part):
    rows_count, seq_total = real_part.shape
    second_len = seq_total // FIRST_LEN
    cos_first, sin_first = dft_tables(FIRST_LEN, FIRST_LEN, FIRST_LEN)
    cos_twist, sin_twist = dft_tables(FIRST_LEN, second_len, seq_total)
    cos_second, sin_second = dft_tables(second_len, second_len, second_len)
    real_cube = real_part.reshape(rows_count, FIRST_LEN, second_len)
    imag_cube = imag_part.reshape(rows_count, FIRST_LEN, second_len)
    section_real = transform_first(real_cube, cos_first) + transform_first(imag_cube, sin_first)
    section_imag = transform_first(imag_cube, cos_first) - transform_first(real_cube, sin_first)
    twist_real = section_real * cos_twist + section_imag * sin_twist
    twist_imag = section_imag * cos_twist - section_real * sin_twist
    summed = transform_second(twist_real, cos_second) + transform_second(twist_imag, sin_second)
    norm_scale = 1.0 / jnp.sqrt(jnp.float32(seq_total * GROUP_WIDTH))
    return (summed.reshape(rows_count, seq_total) * norm_scale).astype(jnp.bfloat16)


def on_device(tokens, norm_gain, w_fourier_in, w_gate, w_spectrum, w_output):
    batches, seq_local, features = tokens.shape
    tokens_count = batches * seq_local
    widened = tokens.astype(jnp.float32)
    inverse = lax.rsqrt(jnp.mean(widened * widened, axis=-1, keepdims=True) + norm_eps)
    normed = (widened * inverse * norm_gain).astype(jnp.bfloat16).reshape(tokens_count, features)
    fourier_in = jnp.dot(normed, w_fourier_in, preferred_element_type=jnp.float32).astype(
        jnp.bfloat16
    )
    local_groups = w_fourier_in.shape[1] // GROUP_WIDTH
    grouped = fourier_in.astype(jnp.float32).reshape(batches, seq_local, local_groups, GROUP_WIDTH)
    cos_group, sin_group = dft_tables(GROUP_WIDTH, GROUP_WIDTH, GROUP_WIDTH)
    real_part = jnp.einsum(
        "btgn,nm->bgmt", grouped, cos_group, precision=lax.Precision.HIGHEST
    ).reshape(-1, seq_local)
    imag_part = -jnp.einsum(
        "btgn,nm->bgmt", grouped, sin_group, precision=lax.Precision.HIGHEST
    ).reshape(-1, seq_local)
    real_part = lax.all_to_all(
        shortened(real_part), "row", split_axis=0, concat_axis=1, tiled=True
    ).astype(real_part.dtype)
    imag_part = lax.all_to_all(
        shortened(imag_part), "row", split_axis=0, concat_axis=1, tiled=True
    ).astype(imag_part.dtype)
    spectrum = positional(real_part, imag_part)
    spectrum = lax.all_to_all(spectrum, "row", split_axis=1, concat_axis=0, tiled=True)
    spectrum = spectrum.reshape(batches, local_groups * GROUP_WIDTH, seq_local)
    spectrum = jnp.transpose(spectrum, (0, 2, 1)).reshape(tokens_count, local_groups * GROUP_WIDTH)

    def add_spectrum(running, portion, beginning):
        weight_rows = lax.dynamic_slice_in_dim(w_spectrum, beginning, portion.shape[1], 0)
        return running + jnp.dot(portion, weight_rows, preferred_element_type=jnp.float32)

    mixed_pre = over_all(
        spectrum, "col", 1, add_spectrum, jnp.zeros((tokens_count, features), jnp.float32)
    ).astype(jnp.bfloat16)
    gate_pre = jnp.dot(normed, w_gate, preferred_element_type=jnp.float32)
    mixed = (jax.nn.sigmoid(gate_pre) * mixed_pre.astype(jnp.float32)).astype(jnp.bfloat16)
    result = jnp.dot(mixed, w_output, preferred_element_type=jnp.float32)
    return result.astype(jnp.bfloat16).reshape(batches, seq_local, -1)


MESH = pl.DeviceIdType.MESH
HALF = GROUP_WIDTH // 2


def channel_tables():
    n = np.arange(GROUP_WIDTH)
    fold = np.zeros((GROUP_WIDTH, GROUP_WIDTH))
    unfold = np.zeros((GROUP_WIDTH, GROUP_WIDTH))
    for d in range(GROUP_WIDTH):
        if d <= HALF:
            fold[:, d] = np.cos(2 * np.pi * (n * d % GROUP_WIDTH) / GROUP_WIDTH)
            unfold[d, d] = 1.0
            unfold[d, (GROUP_WIDTH - d) % GROUP_WIDTH] = 1.0
        else:
            m = d - HALF
            fold[:, d] = np.sin(2 * np.pi * (n * m % GROUP_WIDTH) / GROUP_WIDTH)
            unfold[d, m] = -1.0
            unfold[d, GROUP_WIDTH - m] = 1.0
    return fold, unfold


def position_tables(n):
    a = np.arange(n)
    ang = 2 * np.pi * (np.outer(a, a) % n) / n
    first = np.concatenate([np.cos(ang), np.sin(ang)], 0)
    second = np.concatenate([np.cos(ang), np.sin(ang)], 1)
    phi = 2 * np.pi * np.outer(a, a) / (n * n)
    scale = 1.0 / np.sqrt(n * n * GROUP_WIDTH)
    c, s = np.cos(phi) * scale, np.sin(phi) * scale
    twist = np.stack([np.stack([c, s]), np.stack([s, -c])])
    return first, second, twist


def mixer_kernel(
    rows, cols, tok, gain, wp, wg, ws, wo, f1, f2, tw, out,
    tokv, wgv, gate, inv, ysc, osc, s1, x1, s2, spec,
    tsem, wsem, s1s, s1r, s2s, spr, fws,
):
    batches, seq_local, features = tok.shape
    cpd, steps, n = x1.shape[2:]
    me = lax.axis_index("row")
    col = lax.axis_index("col")
    sib = col + 1 - 2 * lax.rem(col, 2)
    chips = cols // 2
    chunk = 4 * n
    chunks = seq_local // chunk

    def peer(i):
        return lax.rem(me + i, rows)

    def xpeer(j):
        return lax.rem(col + 2 * j, cols)

    loads = {}
    for b in range(batches):
        for j in range(chunks):
            part = pl.ds(j * chunk, chunk)
            loads[b, j] = pltpu.make_async_copy(
                tok.at[b, part], tokv.at[b, part], tsem.at[b, j]
            )
            loads[b, j].start()
    wload = pltpu.make_async_copy(wg, wgv, wsem)
    wload.start()

    barrier = pltpu.get_barrier_semaphore()
    for i in range(1, rows):
        pl.semaphore_signal(barrier, inc=1, device_id={"row": peer(i)}, device_id_type=MESH)
    for j in range(1, chips):
        pl.semaphore_signal(barrier, inc=1, device_id={"col": xpeer(j)}, device_id_type=MESH)
    pl.semaphore_signal(barrier, inc=1, device_id={"col": sib}, device_id_type=MESH)

    def project(b):
        for j in range(chunks):
            loads[b, j].wait()
            t = tokv[b, j * chunk:(j + 1) * chunk, :]
            w = t.astype(jnp.float32)
            scale = lax.rsqrt(jnp.mean(w * w, axis=-1, keepdims=True) + norm_eps)
            inv[b, j * chunk:(j + 1) * chunk, :] = scale
            y = jnp.dot(t, wp[...], preferred_element_type=jnp.float32) * scale
            for k in range(4):
                ysc[:, 4 * j + k, :] = y[k * n:(k + 1) * n, :].T
        s1[b] = ysc[...].astype(jnp.bfloat16)

    def first_copy(b, i, src):
        to = peer(i)
        return pltpu.make_async_remote_copy(
            src_ref=s1.at[b, pl.ds(to * cpd, cpd)],
            dst_ref=x1.at[b, src],
            send_sem=s1s.at[b, i],
            recv_sem=s1r.at[b, src],
            device_id={"row": to},
            device_id_type=MESH,
        )

    def send_first(b):
        for i in ORDER(rows):
            first_copy(b, i, me).start()
        x1[b, me] = s1[b, pl.ds(me * cpd, cpd)]

    def wait_first(b):
        for i in range(1, rows):
            first_copy(b, i, peer(i)).wait_recv()

    def gates(b, j):
        part = slice(j * chunk, (j + 1) * chunk)
        g = jnp.dot(tokv[b, part, :], wgv[...], preferred_element_type=jnp.float32)
        half = 0.5 * inv[b, part, :]
        gate[b, part, :] = (0.5 * jnp.tanh(g * half) + 0.5).astype(jnp.bfloat16)

    def transform(b):
        for c in range(cpd):
            kind = (lax.rem(me * cpd + c, GROUP_WIDTH) > HALF).astype(jnp.int32)
            x = x1[b, :, c].reshape(n, n)
            g = jnp.dot(f1[...], x, preferred_element_type=jnp.float32)
            ca, sa = tw[kind, 0], tw[kind, 1]
            u = g[:n] * ca - g[n:] * sa
            v = -(g[:n] * sa + g[n:] * ca)
            t = jnp.concatenate([u.astype(jnp.bfloat16), v.astype(jnp.bfloat16)], axis=1)
            o = lax.dot_general(
                f2[...], t, (((1,), (1,)), ((), ())), preferred_element_type=jnp.float32
            )
            osc[:, c, :] = o
        s2[b] = osc[...].astype(jnp.bfloat16)

    def second_copy(b, i, src):
        to = peer(i)
        return pltpu.make_async_remote_copy(
            src_ref=s2.at[b, pl.ds(to * steps, steps)],
            dst_ref=spec.at[col, b, src],
            send_sem=s2s.at[b, i],
            recv_sem=spr.at[col, b, src],
            device_id={"row": to},
            device_id_type=MESH,
        )

    def send_second(b):
        for i in ORDER(rows):
            second_copy(b, i, me).start()
        spec[col, b, me] = s2[b, pl.ds(me * steps, steps)]

    def share(b, src, owner, slot, to):
        return pltpu.make_async_remote_copy(
            src_ref=spec.at[owner, b, src],
            dst_ref=spec.at[owner, b, src],
            send_sem=fws.at[slot, b, src],
            recv_sem=spr.at[owner, b, src],
            device_id={"col": to},
            device_id_type=MESH,
        )

    def relay_own(b, i):
        src = peer(i)
        if i > 0:
            second_copy(b, i, src).wait_recv()
        for j in range(1, chips):
            share(b, src, col, j - 1, xpeer(j)).start()
        share(b, src, col, chips - 1, sib).start()

    def relay_far(b, i):
        src = peer(i)
        for j in range(1, chips):
            share(b, src, xpeer(j), chips - 1 + j, sib).wait_recv()
            share(b, src, xpeer(j), chips - 1 + j, sib).start()

    def relay_order():
        return [0] + list(RECV(rows))

    def relay(b, i):
        order = relay_order()
        relay_own(b, order[i])
        if i > 1:
            relay_far(b, order[i - 2])

    def relay_tail(b):
        order = relay_order()
        for i in order[-2:]:
            relay_far(b, i)
        for i in order:
            src = peer(i)
            share(b, src, sib, 0, sib).wait_recv()
            for j in range(1, chips):
                share(b, src, lax.rem(sib + 2 * j, cols), 0, sib).wait_recv()

    def finish(b, j):
        part = slice(j * chunk, (j + 1) * chunk)
        pieces = []
        for k in range(4):
            piece = spec[:, b, :, 4 * j + k].reshape(cols * rows * cpd, n)
            pieces.append(piece.T)
        lhs = jnp.concatenate(pieces, axis=0)
        pre = jnp.dot(lhs, ws[...], preferred_element_type=jnp.float32)
        mixed = (gate[b, part, :].astype(jnp.float32) * pre).astype(jnp.bfloat16)
        out[b, part, :] = jnp.dot(
            mixed, wo[...], preferred_element_type=jnp.float32
        ).astype(jnp.bfloat16)

    project(0)
    pl.semaphore_wait(barrier, rows - 1 + chips)
    send_first(0)
    for b in range(1, batches):
        project(b)
        send_first(b)
    wload.wait()
    wgv[...] = (wgv[...].astype(jnp.float32) * gain[...]).astype(jnp.bfloat16)
    for j in range(chunks):
        gates(0, j)
    for b in range(batches):
        wait_first(b)
        transform(b)
        send_second(b)
        if b + 1 < batches:
            for j in range(chunks):
                gates(b + 1, j)
    for i in range(rows):
        relay(0, i)
    relay_tail(0)
    for b in range(batches):
        for j in range(chunks):
            finish(b, j)
            if b + 1 < batches:
                for i in range(j * rows // chunks, (j + 1) * rows // chunks):
                    relay(b + 1, i)
        if b + 1 < batches:
            relay_tail(b + 1)
    for b in range(batches):
        for i in range(1, rows):
            first_copy(b, i, me).wait_send()
            second_copy(b, i, me).wait_send()
        for i in range(rows):
            for slot in range(2 * chips - 1):
                share(b, peer(i), col, slot, sib).wait_send()


def ORDER(rows):
    return range(1, rows)


def RECV(rows):
    return range(rows - 1, 0, -1)


def fused(rows, cols, tokens, norm_gain, w_fourier_in, w_gate, w_spectrum, w_output):
    batches, seq_local, features = tokens.shape
    n = int(round((seq_local * rows) ** 0.5))
    channels = w_fourier_in.shape[1]
    cpd = channels // rows
    steps = seq_local // n
    fold, unfold = channel_tables()
    first, second, twist = position_tables(n)
    local_groups = channels // GROUP_WIDTH
    gained = w_fourier_in.astype(jnp.float32) * norm_gain[:, None]
    wp = jnp.dot(
        gained,
        jnp.asarray(np.kron(np.eye(local_groups), fold), jnp.float32),
        precision=lax.Precision.HIGHEST,
    ).astype(jnp.bfloat16)
    ws = jnp.einsum(
        "dm,gmj->gdj",
        jnp.asarray(unfold, jnp.bfloat16),
        w_spectrum.reshape(-1, GROUP_WIDTH, features),
        preferred_element_type=jnp.float32,
    ).astype(jnp.bfloat16).reshape(-1, features)
    vmem = pl.BlockSpec(memory_space=pltpu.VMEM)
    hbm = pl.BlockSpec(memory_space=pl.ANY)
    chunks = seq_local // (4 * n)
    dma = pltpu.SemaphoreType.DMA
    return pl.pallas_call(
        functools.partial(mixer_kernel, rows, cols),
        out_shape=jax.ShapeDtypeStruct((batches, seq_local, w_output.shape[1]), jnp.bfloat16),
        in_specs=[hbm, vmem, vmem, hbm, vmem, vmem, vmem, vmem, vmem],
        out_specs=vmem,
        scratch_shapes=[
            pltpu.VMEM(tokens.shape, jnp.bfloat16),
            pltpu.VMEM((features, features), jnp.bfloat16),
            pltpu.VMEM((batches, seq_local, features), jnp.bfloat16),
            pltpu.VMEM((batches, seq_local, 1), jnp.float32),
            pltpu.VMEM((channels, steps, n), jnp.float32),
            pltpu.VMEM((n, cpd, n), jnp.float32),
            pltpu.VMEM((batches, channels, steps, n), jnp.bfloat16),
            pltpu.VMEM((batches, rows, cpd, steps, n), jnp.bfloat16),
            pltpu.VMEM((batches, n, cpd, n), jnp.bfloat16),
            pltpu.VMEM((cols, batches, rows, steps, cpd, n), jnp.bfloat16),
            dma((batches, chunks)),
            dma(()),
            dma((batches, rows)),
            dma((batches, rows)),
            dma((batches, rows)),
            dma((cols, batches, rows)),
            dma((cols, batches, rows)),
        ],
        compiler_params=pltpu.CompilerParams(
            collective_id=0, has_side_effects=True, vmem_limit_bytes=60 * 1024 * 1024
        ),
    )(
        tokens, norm_gain[:, None], wp, w_gate, ws, w_output,
        jnp.asarray(first, jnp.bfloat16), jnp.asarray(second, jnp.bfloat16),
        jnp.asarray(twist, jnp.float32),
    )


def body(rows, cols, *args):
    tokens, w_fourier_in = args[0], args[2]
    seq_local, channels = tokens.shape[1], w_fourier_in.shape[1]
    n = int(round((seq_local * rows) ** 0.5))
    fits = (
        n * n == seq_local * rows
        and n % 128 == 0
        and channels % (16 * rows) == 0
        and channels % GROUP_WIDTH == 0
        and seq_local % (16 * n) == 0
        and cols % 2 == 0
    )
    if fits:
        return fused(rows, cols, *args)
    return on_device(*args)


def solution(mesh):
    placed = (P(None, "row", None), P(), P(None, "col"), P(), P(), P(None, "col"))
    return jax.shard_map(
        functools.partial(body, mesh.shape["row"], mesh.shape["col"]),
        mesh=mesh, in_specs=placed, out_specs=P(None, "row", "col"), check_vma=False,
    )
```

profile of v0, /device:TPU:25, one launch (start us, length us, event | category | flops | bytes accessed | tf_op | source)
XLA Modules:
  0.0 89.4 jit_solution(1107665008368144572)
XLA Ops:
  0.0 0.0 copy-start
  0.0 1.2 %copy-done = bf16[512,1024]{1,0:T(8,128)(2,1)S(1)} copy-done((bf16[512,1024]{1,0:T(8,128)(2,1)S(1)}, bf16[512,1024]{1,0:T(8,128)(2,1)}, u32[]{:S(2)}) %copy-start) | copy-done | bytes 1048600
  1.2 2.3 %convolution_convert_fusion.1.wp = bf16[1024,128]{1,0:T(8,128)(2,1)} fusion(f32[128,128]{1,0:T(8,128)} %constant.10.clone, bf16[1024,128]{1,0:T(8,128)(2,1)} %param.13, f32[1024]{0:T(1024)} %param.12), kind=kOutput, calls=%fused_computation.1 | convolution fusion | flops 201719808 | bytes 593920 | tf_op jit(solution)/shard_map/dot_general | solution.py:352
  3.5 1.7 %copy.12.gain = f32[1024,1]{1,0:T(8,128)} copy(f32[1024,1]{0,1:T(1,128)} %bitcast.11) | data formatting | bytes 8192 | tf_op jit(solution)/shard_map/broadcast_in_dim | solution.py:395
  5.2 2.1 %convolution_convert_fusion = bf16[64,8,1024]{2,0,1:T(8,128)(2,1)} fusion(bf16[64,64,1]{1,0,2:T(8,128)(2,1)} %constant.15, bf16[8,64,1024]{2,1,0:T(8,128)(2,1)S(1)} %bitcast.9), kind=kOutput, calls=%fused_computation | convolution fusion | flops 67633152 | bytes 2105344 | tf_op jit(solution)/shard_map/dm,gmj->gdj/dot_general | solution.py:357
  7.3 79.0 %shard_map.109 = bf16[2,2048,256]{2,1,0:T(8,128)(2,1)} custom-call(bf16[2,2048,1024]{2,1,0:T(8,128)(2,1)} %tok.1, f32[1024,1]{1,0:T(8,128)} %copy.12.gain, bf16[1024,128]{1,0:T(8,128)(2,1)} %convolution_convert_fusion.1.wp, bf16[1024,1024]{1,0:T(8,128)(2,1)} %wg.1, bf16[512,1024]{1,0:T(8,128)(2,1)} %bitcast.10, bf16[1024,256]{1,0:T(8,128)(2,1)} %wo.1, ...), custom_call_target="tpu_custom_call" | custom-call | tf_op jit(solution)/shard_map/pallas_call | solution.py:367
  86.4 3.0 %copy.14 = bf16[2,2048,256]{2,1,0:T(8,128)(2,1)} copy(bf16[2,2048,256]{2,1,0:T(8,128)(2,1)} %shard_map.109) | data formatting | bytes 4194304
Async XLA Ops:
  0.0 1.2 %copy-start = (bf16[512,1024]{1,0:T(8,128)(2,1)S(1)}, bf16[512,1024]{1,0:T(8,128)(2,1)}, u32[]{:S(2)}) copy-start(bf16[512,1024]{1,0:T(8,128)(2,1)} %param.15) | copy-start | bytes 3145732
where the time goes:
time: 89.7 us; the launch traced here: 89.4 us
  Pallas kernels  79 us (88%)
  local copies, waits for them, and re-layouts  5.98 us (7%)
  matrix products  4.41 us (5%)
    pallas_call x1, Pallas kernels, fused(): pl.pallas_call(functools.partial(mixer_kernel, rows, cols), out_shape=jax...  79 us
    unnamed x3, local copies, waits for them, and re-layouts  4.27 us
    dot_general x1, matrix products, fused(): jnp.dot(gained, jnp.asarray(np.kron(np.eye(local_groups), fold), jnp.floa...  2.31 us
    dot_general x1, matrix products, fused(): jnp.einsum('dm,gmj->gdj', jnp.asarray(unfold, jnp.bfloat16), w_spectrum.r...  2.1 us

commit v1 on v0

--- a/solution.py
+++ b/solution.py
@@ -132,8 +132,8 @@
 
 
 def mixer_kernel(
-    rows, cols, tok, gain, wp, wg, ws, wo, f1, f2, tw, out,
-    tokv, wgv, gate, inv, ysc, osc, s1, x1, s2, spec,
+    rows, cols, tok, gain, wf, wg, wspec, wout, fold, unfold, f1, f2, tw, out,
+    tokv, wgv, wsv, ws, wo, wp, gate, inv, ysc, osc, s1, x1, s2, spec,
     tsem, wsem, s1s, s1r, s2s, spr, fws,
 ):
     batches, seq_local, features = tok.shape
@@ -159,8 +159,12 @@
                 tok.at[b, part], tokv.at[b, part], tsem.at[b, j]
             )
             loads[b, j].start()
-    wload = pltpu.make_async_copy(wg, wgv, wsem)
+    wload = pltpu.make_async_copy(wg, wgv, wsem.at[0])
     wload.start()
+    sload = pltpu.make_async_copy(wspec, wsv, wsem.at[1])
+    sload.start()
+    oload = pltpu.make_async_copy(wout, wo, wsem.at[2])
+    oload.start()
 
     barrier = pltpu.get_barrier_semaphore()
     for i in range(1, rows):
@@ -168,6 +172,16 @@
     for j in range(1, chips):
         pl.semaphore_signal(barrier, inc=1, device_id={"col": xpeer(j)}, device_id_type=MESH)
     pl.semaphore_signal(barrier, inc=1, device_id={"col": sib}, device_id_type=MESH)
+
+    gained = []
+    lanes = 128
+    for k in range(features // lanes):
+        column = jnp.broadcast_to(gain[:, k * lanes:(k + 1) * lanes], (lanes, lanes)).T
+        gained.append(column)
+        w = wf[k * lanes:(k + 1) * lanes, :].astype(jnp.float32) * column[:, :1]
+        wp[k * lanes:(k + 1) * lanes, :] = jnp.dot(
+            w, fold[...], precision=lax.Precision.HIGHEST, preferred_element_type=jnp.float32
+        ).astype(jnp.bfloat16)
 
     def project(b):
         for j in range(chunks):
@@ -301,9 +315,19 @@
         project(b)
         send_first(b)
     wload.wait()
-    wgv[...] = (wgv[...].astype(jnp.float32) * gain[...]).astype(jnp.bfloat16)
+    for k in range(features // lanes):
+        part = slice(k * lanes, (k + 1) * lanes)
+        scaled = wgv[part, :].astype(jnp.float32) * gained[k][:, :1]
+        wgv[part, :] = scaled.astype(jnp.bfloat16)
     for j in range(chunks):
         gates(0, j)
+    sload.wait()
+    for k in range(wsv.shape[0] // GROUP_WIDTH):
+        part = slice(k * GROUP_WIDTH, (k + 1) * GROUP_WIDTH)
+        ws[part, :] = jnp.dot(
+            unfold[...], wsv[part, :], preferred_element_type=jnp.float32
+        ).astype(jnp.bfloat16)
+    oload.wait()
     for b in range(batches):
         wait_first(b)
         transform(b)
@@ -348,18 +372,6 @@
     fold, unfold = channel_tables()
     first, second, twist = position_tables(n)
     local_groups = channels // GROUP_WIDTH
-    gained = w_fourier_in.astype(jnp.float32) * norm_gain[:, None]
-    wp = jnp.dot(
-        gained,
-        jnp.asarray(np.kron(np.eye(local_groups), fold), jnp.float32),
-        precision=lax.Precision.HIGHEST,
-    ).astype(jnp.bfloat16)
-    ws = jnp.einsum(
-        "dm,gmj->gdj",
-        jnp.asarray(unfold, jnp.bfloat16),
-        w_spectrum.reshape(-1, GROUP_WIDTH, features),
-        preferred_element_type=jnp.float32,
-    ).astype(jnp.bfloat16).reshape(-1, features)
     vmem = pl.BlockSpec(memory_space=pltpu.VMEM)
     hbm = pl.BlockSpec(memory_space=pl.ANY)
     chunks = seq_local // (4 * n)
@@ -367,11 +379,15 @@
     return pl.pallas_call(
         functools.partial(mixer_kernel, rows, cols),
         out_shape=jax.ShapeDtypeStruct((batches, seq_local, w_output.shape[1]), jnp.bfloat16),
-        in_specs=[hbm, vmem, vmem, hbm, vmem, vmem, vmem, vmem, vmem],
+        in_specs=[hbm, vmem, vmem, hbm, hbm, hbm, vmem, vmem, vmem, vmem, vmem],
         out_specs=vmem,
         scratch_shapes=[
             pltpu.VMEM(tokens.shape, jnp.bfloat16),
             pltpu.VMEM((features, features), jnp.bfloat16),
+            pltpu.VMEM(w_spectrum.shape, jnp.bfloat16),
+            pltpu.VMEM(w_spectrum.shape, jnp.bfloat16),
+            pltpu.VMEM(w_output.shape, jnp.bfloat16),
+            pltpu.VMEM(w_fourier_in.shape, jnp.bfloat16),
             pltpu.VMEM((batches, seq_local, features), jnp.bfloat16),
             pltpu.VMEM((batches, seq_local, 1), jnp.float32),
             pltpu.VMEM((channels, steps, n), jnp.float32),
@@ -381,7 +397,7 @@
             pltpu.VMEM((batches, n, cpd, n), jnp.bfloat16),
             pltpu.VMEM((cols, batches, rows, steps, cpd, n), jnp.bfloat16),
             dma((batches, chunks)),
-            dma(()),
+            dma((3,)),
             dma((batches, rows)),
             dma((batches, rows)),
             dma((batches, rows)),
@@ -389,10 +405,12 @@
             dma((cols, batches, rows)),
         ],
         compiler_params=pltpu.CompilerParams(
-            collective_id=0, has_side_effects=True, vmem_limit_bytes=60 * 1024 * 1024
+            collective_id=0, has_side_effects=True, vmem_limit_bytes=44 * 1024 * 1024
         ),
     )(
-        tokens, norm_gain[:, None], wp, w_gate, ws, w_output,
+        tokens, norm_gain[None, :], w_fourier_in, w_gate, w_spectrum, w_output,
+        jnp.asarray(np.kron(np.eye(local_groups), fold), jnp.float32),
+        jnp.asarray(unfold, jnp.bfloat16),
         jnp.asarray(first, jnp.bfloat16), jnp.asarray(second, jnp.bfloat16),
         jnp.asarray(twist, jnp.float32),
     )

time: 89.7 us -> 87.7 us (0.978)
  local copies, waits for them, and re-layouts: 5.98 us -> 11 us
  matrix products: 4.41 us -> 0 us
  Pallas kernels: 79 us -> 76.1 us
    unnamed x3 -> x21, local copies, waits for them, and re-layouts: 4.27 us -> 11 us
    dot_general x2 -> x0, matrix products: 4.41 us -> none  [the longest x1 2.31 us: fused(): jnp.dot(gained, jnp.asarray(np.kron(np.eye(local_groups), fold), jnp.floa...]
    pallas_call x1, Pallas kernels: 79 us -> 76.1 us  [fused(): pl.pallas_call(functools.partial(mixer_kernel, rows, cols), out_shape=jax...]
    broadcast_in_dim x1 -> x0, local copies, waits for them, and re-layouts: 1.71 us -> none  [fused(): norm_gain[:, None]]
where the time goes in v1:
time: 87.7 us; the launch traced here: 87.2 us
  Pallas kernels  76.1 us (87%)
  local copies, waits for them, and re-layouts  11 us (13%)
    pallas_call x1, Pallas kernels, fused(): pl.pallas_call(functools.partial(mixer_kernel, rows, cols), out_shape=jax...  76.1 us
    unnamed x21, local copies, waits for them, and re-layouts  11 us

profile of v1, /device:TPU:25, one launch (start us, length us, event | category | flops | bytes accessed | tf_op | source)
XLA Modules:
  0.0 87.2 jit_solution(2461423457422091875)
XLA Ops:
  0.0 0.0 copy-start
  0.0 1.6 %copy-done = bf16[1024,1024]{1,0:T(8,128)(2,1)S(1)} copy-done((bf16[1024,1024]{1,0:T(8,128)(2,1)S(1)}, bf16[1024,1024]{1,0:T(8,128)(2,1)}, u32[]{:S(2)}) %copy-start) | copy-done | bytes 2097176
  1.6 0.0 copy-start.1
  1.6 1.2 %copy-done.1 = bf16[512,1024]{1,0:T(8,128)(2,1)S(1)} copy-done((bf16[512,1024]{1,0:T(8,128)(2,1)S(1)}, bf16[512,1024]{1,0:T(8,128)(2,1)}, u32[]{:S(2)}) %copy-start.1) | copy-done | bytes 1048600
  2.8 0.0 copy-start.2
  2.8 1.0 %copy-done.2 = bf16[1024,256]{1,0:T(8,128)(2,1)S(1)} copy-done((bf16[1024,256]{1,0:T(8,128)(2,1)S(1)}, bf16[1024,256]{1,0:T(8,128)(2,1)}, u32[]{:S(2)}) %copy-start.2) | copy-done | bytes 524312
  3.9 0.0 copy-start.3
  3.9 0.9 %copy-done.3 = bf16[1024,128]{1,0:T(8,128)(2,1)S(1)} copy-done((bf16[1024,128]{1,0:T(8,128)(2,1)S(1)}, bf16[1024,128]{1,0:T(8,128)(2,1)}, u32[]{:S(2)}) %copy-start.3) | copy-done | bytes 262168
  4.8 0.0 copy-start.4
  4.8 0.9 %copy-done.4 = f32[2,2,128,128]{3,2,1,0:T(8,128)S(1)} copy-done((f32[2,2,128,128]{3,2,1,0:T(8,128)S(1)}, f32[2,2,128,128]{3,2,1,0:T(8,128)}, u32[]{:S(2)}) %copy-start.4) | copy-done | bytes 262168
  5.8 0.0 copy-start.5
  5.8 0.8 copy-done.5
  6.6 0.0 copy-start.6
  6.6 0.8 copy-done.6
  7.4 0.0 copy-start.7
  7.4 0.8 copy-done.7
  8.3 0.0 copy-start.8
  8.3 0.7 copy-done.8
  9.0 0.0 copy-start.9
  9.0 0.7 copy-done.9
  9.7 76.1 %shard_map.109 = bf16[2,2048,256]{2,1,0:T(8,128)(2,1)S(1)} custom-call(bf16[2,2048,1024]{2,1,0:T(8,128)(2,1)} %tok.1, f32[1,1024]{1,0:T(1,128)S(1)} %bitcast.1, bf16[1024,128]{1,0:T(8,128)(2,1)S(1)} %copy-done.3, bf16[1024,1024]{1,0:T(8,128)(2,1)S(1)} %copy-done, bf16[512,1024]{1,0:T(8,128)(2,1)S(1)} %copy-done.1, bf16[1024,256]{1,0:T(8,128)(2,1)S(1)} %copy-done.2, ...), custom_call_target="tpu_custom_call" | custom-call | tf_op jit(solution)/shard_map/pallas_call | solution.py:379
  85.8 1.3 %copy.13 = bf16[2,2048,256]{2,1,0:T(8,128)(2,1)} copy(bf16[2,2048,256]{2,1,0:T(8,128)(2,1)S(1)} %shard_map.109) | data formatting | bytes 4194304
Async XLA Ops:
  0.0 1.6 %copy-start = (bf16[1024,1024]{1,0:T(8,128)(2,1)S(1)}, bf16[1024,1024]{1,0:T(8,128)(2,1)}, u32[]{:S(2)}) copy-start(bf16[1024,1024]{1,0:T(8,128)(2,1)} %wg.1) | copy-start | bytes 6291460
  1.6 1.2 %copy-start.1 = (bf16[512,1024]{1,0:T(8,128)(2,1)S(1)}, bf16[512,1024]{1,0:T(8,128)(2,1)}, u32[]{:S(2)}) copy-start(bf16[512,1024]{1,0:T(8,128)(2,1)} %wspec.1) | copy-start | bytes 3145732
  2.8 1.0 %copy-start.2 = (bf16[1024,256]{1,0:T(8,128)(2,1)S(1)}, bf16[1024,256]{1,0:T(8,128)(2,1)}, u32[]{:S(2)}) copy-start(bf16[1024,256]{1,0:T(8,128)(2,1)} %wout.1) | copy-start | bytes 1572868
  3.9 0.9 %copy-start.3 = (bf16[1024,128]{1,0:T(8,128)(2,1)S(1)}, bf16[1024,128]{1,0:T(8,128)(2,1)}, u32[]{:S(2)}) copy-start(bf16[1024,128]{1,0:T(8,128)(2,1)} %wf.1) | copy-start | bytes 786436
  4.8 0.9 %copy-start.4 = (f32[2,2,128,128]{3,2,1,0:T(8,128)S(1)}, f32[2,2,128,128]{3,2,1,0:T(8,128)}, u32[]{:S(2)}) copy-start(f32[2,2,128,128]{3,2,1,0:T(8,128)} %constant.14.clone.tw) | copy-start | bytes 786436
  5.8 0.8 copy-start.5
  6.6 0.8 copy-start.6
  7.4 0.8 copy-start.7
  8.3 0.7 copy-start.8
  9.0 0.7 copy-start.9
